TPU v7x, 32 devices: a whole 2x2x4 slice. The times are simulated.
32 devices in a mesh: fs: 8 (over z, x), tp: 4 (over y, core).
Axes of the slice: x: 2, y: 2, z: 4, core: 2. Of those that a mesh axis runs over, the one named last changes fastest.
Arguments:
- normed_inputs: bfloat16 [24576, 2048], P(('fs', 'tp')), may hold values from -6 to 6
- query_cotangent: bfloat16 [24576, 1024], P(('fs', 'tp')), may hold values from -6 to 6
- head_outputs: bfloat16 [24576, 1024], P(('fs', 'tp')), may hold values from -6 to 6
- output_cotangent: bfloat16 [24576, 2048], P(('fs', 'tp')), may hold values from -6 to 6
- query_weight: float32 [2048, 1024], P('fs', 'tp'), may hold values from -0.125 to 0.125
- out_weight: float32 [1024, 2048], P('fs', 'tp'), may hold values from -0.1875 to 0.1875
- query_basis: bfloat16 [2048, 512], P('fs'), may hold values from -0.125 to 0.125
- out_basis: bfloat16 [1024, 512], P('fs'), may hold values from -0.1875 to 0.1875
- query_mean: float32 [512, 1024], P('fs', 'tp'), may hold values from -6 to 6
- query_square: float32 [512, 1024], P('fs', 'tp'), may hold values from 0.5 to 2
- out_mean: float32 [512, 2048], P('fs', 'tp'), may hold values from -6 to 6
- out_square: float32 [512, 2048], P('fs', 'tp'), may hold values from 0.5 to 2
Outputs:
- query_mean_new: float32 [512, 1024], P('fs', 'tp')
- query_square_new: float32 [512, 1024], P('fs', 'tp')
- query_step: float32 [2048, 1024], P('fs', 'tp')
- query_weight_new: float32 [2048, 1024], P('fs', 'tp')
- query_copy: bfloat16 [2048, 1024], P(None, 'tp')
- out_mean_new: float32 [512, 2048], P('fs', 'tp')
- out_square_new: float32 [512, 2048], P('fs', 'tp')
- out_step: float32 [1024, 2048], P('fs', 'tp')
- out_weight_new: float32 [1024, 2048], P('fs', 'tp')
- out_copy: bfloat16 [1024, 2048], P(None, 'tp')
All inputs are finite; a program needn't handle non-finite values.
Results may differ from a plain program's by a relative error of at most 0.009.
Values may be sent and summed in bfloat16 or wider, within the bound.
A program may use at most 64 MiB of HBM per device.

v0:
```python
import jax
import jax.numpy as jnp
from jax import lax
from jax.sharding import PartitionSpec as P


def moments(reduced, mean, square):
    mean_new = 0.8 * mean + 0.2 * reduced
    square_new = 0.9 * square + 0.1 * reduced * reduced
    direction = mean_new / (jnp.sqrt(square_new) + 1e-08)
    return (mean_new, square_new, direction)


def split_product(left, right):
    contract = (((0,), (0,)), ((), ()))
    high = left.astype(jnp.bfloat16)
    low = (left - high.astype(jnp.float32)).astype(jnp.bfloat16)
    return lax.dot_general(
        high, right, contract, preferred_element_type=jnp.float32
    ) + lax.dot_general(low, right, contract, preferred_element_type=jnp.float32)


def shards(
    normed_inputs,
    query_cotangent,
    head_outputs,
    output_cotangent,
    query_weight,
    out_weight,
    query_basis,
    out_basis,
    query_mean,
    query_square,
    out_mean,
    out_square,
):
    fs_count = lax.axis_size("fs")
    tp_count = lax.axis_size("tp")
    model_rows = normed_inputs.shape[1]
    query_width = query_cotangent.shape[1]
    token_scale = (normed_inputs.shape[0] * fs_count * tp_count) ** (-0.5)
    query_cols = query_weight.shape[1]
    out_cols = out_weight.shape[1]
    rank_rows = query_mean.shape[0]
    query_all, out_all = (
        lax.all_gather(query_basis, "fs", axis=0, tiled=True),
        lax.all_gather(out_basis, "fs", axis=0, tiled=True),
    )
    query_left = jnp.dot(normed_inputs, query_all, preferred_element_type=jnp.float32)
    out_left = jnp.dot(head_outputs, out_all, preferred_element_type=jnp.float32)
    query_part = split_product(query_left, query_cotangent)
    out_part = split_product(out_left, output_cotangent)
    reduced = lax.psum_scatter(
        jnp.concatenate(
            [
                query_part.reshape(rank_rows * lax.axis_size("fs"), tp_count, query_cols),
                out_part.reshape(rank_rows * lax.axis_size("fs"), tp_count, out_cols),
            ],
            axis=2,
        ).astype(jnp.bfloat16),
        "fs",
        scatter_dimension=0,
        tiled=True,
    )
    summed = lax.psum_scatter(reduced, "tp", scatter_dimension=1, tiled=True).astype(jnp.float32)
    projected = summed[:, 0, :]
    projected = projected * token_scale
    query_reduced = projected[:, :query_cols]
    out_reduced = projected[:, query_cols:]
    query_mean_new, query_square_new, query_direction = moments(
        query_reduced, query_mean, query_square
    )
    out_mean_new, out_square_new, out_direction = moments(out_reduced, out_mean, out_square)
    query_piece = lax.all_gather(query_direction, "fs", axis=0, tiled=True)
    out_piece = lax.all_gather(out_direction, "fs", axis=0, tiled=True)
    query_part = query_basis.astype(jnp.float32)
    out_part = out_basis.astype(jnp.float32)
    query_full = jnp.dot(query_part, query_piece, precision=lax.Precision.HIGHEST)
    out_full = jnp.dot(out_part, out_piece, precision=lax.Precision.HIGHEST)
    query_norms, out_norms = lax.psum(
        (jnp.sum(query_full * query_full, axis=0), jnp.sum(out_full * out_full, axis=0)), "fs"
    )
    query_step = query_full * lax.rsqrt(query_norms / model_rows + 0.05)
    out_step = out_full * lax.rsqrt(out_norms / query_width + 0.05)
    query_weight_new = query_weight - 0.01 * query_step
    out_weight_new = out_weight - 0.01 * out_step
    query_copy, out_copy = (
        lax.all_gather(query_weight_new.astype(jnp.bfloat16), "fs", axis=0, tiled=True),
        lax.all_gather(out_weight_new.astype(jnp.bfloat16), "fs", axis=0, tiled=True),
    )
    return (
        query_mean_new,
        query_square_new,
        query_step,
        query_weight_new,
        query_copy,
        out_mean_new,
        out_square_new,
        out_step,
        out_weight_new,
        out_copy,
    )


def solution(mesh):
    in_specs = (
        P(("fs", "tp"), None),
        P(("fs", "tp"), None),
        P(("fs", "tp"), None),
        P(("fs", "tp"), None),
        P("fs", "tp"),
        P("fs", "tp"),
        P("fs", None),
        P("fs", None),
        P("fs", "tp"),
        P("fs", "tp"),
        P("fs", "tp"),
        P("fs", "tp"),
    )
    out_specs = (
        P("fs", "tp"),
        P("fs", "tp"),
        P("fs", "tp"),
        P("fs", "tp"),
        P(None, "tp"),
        P("fs", "tp"),
        P("fs", "tp"),
        P("fs", "tp"),
        P("fs", "tp"),
        P(None, "tp"),
    )
    return jax.shard_map(shards, mesh=mesh, in_specs=in_specs, out_specs=out_specs, check_vma=False)
```

profile of v0, /device:TPU:0, one launch (start us, length us, event | category | flops | bytes accessed | tf_op | source)
XLA Modules:
  0.0 366.5 jit_solution(16840274893185502602)
XLA Ops:
  8.7 44.4 %all-gather.8.cloned.1.call-done = bf16[1024,512]{1,0:T(8,128)(2,1)} async-done(((bf16[128,512]{1,0:T(8,128)(2,1)}), bf16[1024,512]{1,0:T(8,128)(2,1)}) %all-gather.8.cloned.1.call-update) | async-done | bytes 1048592 | tf_op jit(solution)/shard_map/all_gather | solution.py:47
  53.2 2.7 fusion.13
  55.8 1.8 fusion.1
  57.7 1.8 add_convert_fusion
  59.5 1.5 copy.28
  61.0 42.1 %all-gather.6.cloned.1.call-done = bf16[2048,512]{1,0:T(8,128)(2,1)} async-done(((bf16[256,512]{1,0:T(8,128)(2,1)}), bf16[2048,512]{1,0:T(8,128)(2,1)}) %all-gather.6.cloned.1.call-update) | async-done | bytes 2097168 | tf_op jit(solution)/shard_map/all_gather | solution.py:46
  103.1 4.4 %fusion.12 = f32[768,512]{1,0:T(8,128)S(1)} fusion(bf16[768,2048]{1,0:T(8,128)(2,1)} %param.12, bf16[2048,512]{1,0:T(8,128)(2,1)} %all-gather.6.cloned.1.call-done), kind=kOutput, calls=%fused_computation.32 | convolution fusion | flops 1610612736 | bytes 6815744 | tf_op jit(solution)/shard_map/dot_general | solution.py:49
  108.6 1.0 add_convert_fusion.1
  109.7 1.5 copy-done.1
  111.2 1.9 pad_maximum_fusion
  113.1 73.1 %reduce-scatter.3.cloned.1.call-done = bf16[64,4,768]{2,0,1:T(8,128)(2,1)} async-done(((bf16[512,4,768]{2,0,1:T(8,128)(2,1)}), bf16[64,4,768]{2,0,1:T(8,128)(2,1)}) %reduce-scatter.3.cloned.1.call-update) | async-done | bytes 393232 | tf_op jit(solution)/shard_map/reduce_scatter | solution.py:53
  186.3 22.2 %reduce-scatter.5.cloned.1.call-done = bf16[64,1,768]{2,0,1:T(8,128)(2,1)} async-done(((bf16[64,4,768]{2,0,1:T(8,128)(2,1)}), bf16[64,1,768]{2,0,1:T(8,128)(2,1)}) %reduce-scatter.5.cloned.1.call-update) | async-done | bytes 98320 | tf_op jit(solution)/shard_map/reduce_scatter | solution.py:65
  210.1 1.7 add_divide_fusion
  211.9 1.6 add_divide_fusion.1
  213.5 32.6 %all_gather.20 = f32[512,256]{1,0:T(8,128)S(1)} all-gather(f32[64,256]{1,0:T(8,128)S(1)} %get-tuple-element.21), channel_id=1, replica_groups=mesh['fs'=8,'tp'=4] {'fs'}, dimensions={0}, use_global_device_ids=true | all-gather | bytes 589824 | tf_op jit(solution)/shard_map/all_gather | solution.py:74
  246.1 1.1 multiply_reduce_fusion.1
  247.2 6.5 %all-gather.12.cloned.1.call-done = f32[512,512]{1,0:T(8,128)} async-done(((f32[64,512]{1,0:T(8,128)}), f32[512,512]{1,0:T(8,128)}) %all-gather.12.cloned.1.call-update) | async-done | bytes 1048592 | tf_op jit(solution)/shard_map/all_gather | solution.py:75
  253.7 2.4 multiply_reduce_fusion
  256.2 19.1 %all-reduce = (f32[256]{0:T(256)S(1)}, f32[512]{0:T(512)S(1)}) all-reduce(f32[256]{0:T(256)S(1)} %get-tuple-element.24, f32[512]{0:T(512)S(1)} %get-tuple-element.26), channel_id=1, replica_groups=mesh['fs'=8,'tp'=4] {'fs'}, use_global_device_ids=true, to_apply=%region_3.0 | all-reduce | flops 768 | bytes 6144 | tf_op jit(solution)/shard_map/psum | solution.py:80
  275.2 1.9 fusion.8
  277.3 1.8 fusion.9
  279.1 35.5 %all-gather.14.cloned.1.call-done = bf16[1024,512]{1,0:T(8,128)(2,1)} async-done(((bf16[128,512]{1,0:T(8,128)(2,1)}), bf16[1024,512]{1,0:T(8,128)(2,1)}) %all-gather.14.cloned.1.call-update) | async-done | bytes 1048592 | tf_op jit(solution)/shard_map/all_gather | solution.py:89
  314.7 41.7 %all-gather.10.cloned.1.call-done = bf16[2048,256]{1,0:T(8,128)(2,1)} async-done(((bf16[256,256]{1,0:T(8,128)(2,1)}), bf16[2048,256]{1,0:T(8,128)(2,1)}) %all-gather.10.cloned.1.call-update) | async-done | bytes 1048592 | tf_op jit(solution)/shard_map/all_gather | solution.py:88
  356.4 2.4 copy.32
  (35 shorter events, 5.4 us)
Async XLA Ops:
  7.2 48.7 %copy-start = (bf16[768,2048]{1,0:T(8,128)(2,1)S(1)}, bf16[768,2048]{1,0:T(8,128)(2,1)}, u32[]{:S(2)}) copy-start(bf16[768,2048]{1,0:T(8,128)(2,1)} %param.15) | copy-start | bytes 9437188
  7.2 46.0 %all-gather.8.cloned.1.call-start = ((), (), s32[]{:S(2)}) async-start(), calls=%async_computation.3 | async-start | bytes 1179648 | tf_op jit(solution)/shard_map/all_gather | solution.py:47
  7.9 95.2 %all-gather.6.cloned.1.call-start = ((), (), s32[]{:S(2)}) async-start(), calls=%async_computation.2 | async-start | bytes 2359296 | tf_op jit(solution)/shard_map/all_gather | solution.py:46
  8.7 177.5 %reduce-scatter.3.cloned.1.call-start = ((), (), s32[]{:S(2)}) async-start(), calls=%async_computation.4 | async-start | bytes 3538944 | tf_op jit(solution)/shard_map/reduce_scatter | solution.py:53
  103.1 4.4 %copy-start.7 = (bf16[768,1024]{1,0:T(8,128)(2,1)S(1)}, bf16[768,1024]{1,0:T(8,128)(2,1)}, u32[]{:S(2)}) copy-start(bf16[768,1024]{1,0:T(8,128)(2,1)} %param.13) | copy-start | bytes 4718596
  109.6 1.6 copy-start.1
  113.0 133.0 %copy-start.2 = (bf16[256,512]{1,0:T(8,128)(2,1)S(1)}, bf16[256,512]{1,0:T(8,128)(2,1)}, u32[]{:S(2)}) copy-start(bf16[256,512]{1,0:T(8,128)(2,1)} %param.18) | copy-start | bytes 786436
  113.1 140.7 %copy-start.6 = (bf16[128,512]{1,0:T(8,128)(2,1)S(1)}, bf16[128,512]{1,0:T(8,128)(2,1)}, u32[]{:S(2)}) copy-start(bf16[128,512]{1,0:T(8,128)(2,1)} %param.19) | copy-start | bytes 393220
  113.1 95.4 %reduce-scatter.5.cloned.1.call-start = ((), (), s32[]{:S(2)}) async-start(), calls=%async_computation.5 | async-start | bytes 491520 | tf_op jit(solution)/shard_map/reduce_scatter | solution.py:65
  186.2 67.5 %all-gather.12.cloned.1.call-start = ((), (), s32[]{:S(2)}) async-start(), calls=%async_computation.7 | async-start | bytes 1179648 | tf_op jit(solution)/shard_map/all_gather | solution.py:75
  209.4 0.7 copy-start.5
  211.9 102.8 %all-gather.14.cloned.1.call-start = ((), (), s32[]{:S(2)}) async-start(), calls=%async_computation.8 | async-start | bytes 1179648 | tf_op jit(solution)/shard_map/all_gather | solution.py:89
  247.2 30.1 %copy-start.4 = (f32[256,256]{0,1:T(8,128)S(1)}, f32[256,256]{0,1:T(8,128)}, u32[]{:S(2)}) copy-start(f32[256,256]{0,1:T(8,128)} %get-tuple-element.25) | copy-start | bytes 786436
  277.2 79.2 %all-gather.10.cloned.1.call-start = ((), (), s32[]{:S(2)}) async-start(), calls=%async_computation.6 | async-start | bytes 1179648 | tf_op jit(solution)/shard_map/all_gather | solution.py:88
  356.4 2.4 copy-start.3
Sparse Core Ops, SparseCore 0:
  10.1 42.9 all-gather.7
  55.3 47.7 all-gather.5
  113.2 72.9 reduce-scatter.2
  188.5 19.9 reduce-scatter.4
  212.0 41.7 all-gather.11
  277.3 37.2 all-gather.13
  317.3 38.9 all-gather.9
where the time goes:
time: 367 us
  waiting for transfers between devices  267 us (73%)
  blocking collectives  51.6 us (14%)
  matrix products  16.4 us (4%)
  between operations  14.2 us (4%)
  other arithmetic  9.87 us (3%)
  local copies, waits for them, and re-layouts  7.1 us (2%)
    reduce_scatter x1, waiting for transfers between devices, shards(): lax.psum_scatter(jnp.concatenate([query_part.reshape(rank_rows * lax.axis...  73.1 us
    all_gather x1, waiting for transfers between devices, shards(): lax.all_gather(out_basis, 'fs', axis=0, tiled=True)  44.4 us
    all_gather x1, waiting for transfers between devices, shards(): lax.all_gather(query_basis, 'fs', axis=0, tiled=True)  42.1 us
    all_gather x1, waiting for transfers between devices, shards(): lax.all_gather(query_weight_new.astype(jnp.bfloat16), 'fs', axis=0, tiled...  41.7 us
    all_gather x1, waiting for transfers between devices, shards(): lax.all_gather(out_weight_new.astype(jnp.bfloat16), 'fs', axis=0, tiled=T...  35.5 us
    all_gather x1, blocking collectives, shards(): query_piece = lax.all_gather(query_direction, 'fs', axis=0, tiled=True)  32.6 us
    reduce_scatter x1, waiting for transfers between devices, shards(): lax.psum_scatter(reduced, 'tp', scatter_dimension=1, tiled=True)  22.2 us
    psum x1, blocking collectives, shards(): lax.psum((jnp.sum(query_full * query_full, axis=0), jnp.sum(out_full * ou...  19.1 us
  transfers between devices with their start and end apart: 7, of which 7 were waited for; matrix products, arithmetic and copies ran while one was open for 3% of the time, Pallas kernels for 0%

commit v1 on v0

v1 whole, which is shorter than its diff:
```python
import functools

import jax
import jax.numpy as jnp
from jax import lax
from jax.experimental import pallas as pl
from jax.experimental.pallas import tpu as pltpu
from jax.sharding import PartitionSpec as P

MESH = pl.DeviceIdType.MESH
F32 = jnp.float32
BF16 = jnp.bfloat16


def plane(fs_count):
    inner = 1
    while 2 * (2 * inner) ** 2 <= fs_count:
        inner *= 2
    return fs_count // inner, inner


def greet(peers):
    barrier = pltpu.get_barrier_semaphore()
    for peer in peers:
        pl.semaphore_signal(barrier, inc=1, device_id=peer, device_id_type=MESH)
    pl.semaphore_wait(barrier, len(peers))


def remote(src, dst, send, recv, peer):
    return pltpu.make_async_remote_copy(
        src_ref=src, dst_ref=dst, send_sem=send, recv_sem=recv, device_id=peer, device_id_type=MESH
    )


def gather_basis(Z, X, qb, ob, qall, oall, zs, zr, xs, xr, ps, pr):
    f, t = lax.axis_index("fs"), lax.axis_index("tp")
    z, x, c = f // X, lax.rem(f, X), lax.rem(t, 2)
    partner = (f, t + 1 - 2 * c)

    def zpeer(dz):
        return (lax.rem(z + dz, Z) * X + x, t)

    def xpeer(dx):
        return (z * X + lax.rem(x + dx, X), t)

    def source(dz, dx):
        return lax.rem(z + Z - dz, Z) * X + lax.rem(x + X - dx, X)

    greet([zpeer(d) for d in range(1, Z)] + [xpeer(d) for d in range(1, X)] + [partner])
    pairs = ((qb, qall), (ob, oall))
    sent = []

    def half(ref, rows, block, core):
        n = rows // 2
        return ref.at[pl.ds(pl.multiple_of(block * rows + core * n, n), n), :]

    def send(i, dz, dx, send_sem, recv_sem, peer):
        own, full = pairs[i]
        rows = own.shape[0]
        dst = half(full, rows, source(dz, dx), c)
        src = half(own, rows, 0, c) if dz == 0 and dx == 0 else dst
        copy = remote(src, dst, send_sem, recv_sem, peer)
        copy.start()
        sent.append(copy)

    def arrived(i, dz, dx, core, send_sem, recv_sem):
        own, full = pairs[i]
        ref = half(full, own.shape[0], source(dz, dx), core)
        remote(ref, ref, send_sem, recv_sem, partner).wait_recv()

    for dz in range(1, Z):
        for i in range(2):
            send(i, dz=0, dx=0, send_sem=zs.at[i, dz], recv_sem=zr.at[i, dz], peer=zpeer(dz))
    for dz in range(Z):
        for i in range(2):
            if dz:
                arrived(i, dz, 0, c, zs.at[i, dz], zr.at[i, dz])
            for dx in range(1, X):
                send(i, dz, 0, xs.at[i, dz, dx], xr.at[i, dz, dx], xpeer(dx))
            if dz:
                send(i, dz, 0, ps.at[i, dz, 0], pr.at[i, dz, 0], partner)
        if dz == 0:
            for own, full in pairs:
                rows = own.shape[0]
                full[pl.ds(pl.multiple_of(f * rows, rows), rows), :] = own[...]
    for dz in range(Z):
        for dx in range(1, X):
            for i in range(2):
                arrived(i, dz, dx, c, xs.at[i, dz, dx], xr.at[i, dz, dx])
                send(i, dz, dx, ps.at[i, dz, dx], pr.at[i, dz, dx], partner)
    for dz in range(Z):
        for dx in range(X):
            if dz or dx:
                for i in range(2):
                    arrived(i, dz, dx, 1 - c, ps.at[i, dz, dx], pr.at[i, dz, dx])
    for copy in sent:
        copy.wait_send()


def update(
    Z, X, Y, scale,
    parts_q, parts_o, wq, wo, mean_q, square_q, mean_o, square_o,
    dq, do, mq, sq, mo, so, wq_all, wo_all,
    r1q, r1o, s1q, s1o, r2q, r2o, s2q, s2o, r3q, r3o, s3q, s3o, r4q, r4o,
    s1s, s1r, s2s, s2r, s3s, s3r, s4s, s4r, gzs, gzr, gxs, gxr,
):
    f, t = lax.axis_index("fs"), lax.axis_index("tp")
    z, x, c, y = f // X, lax.rem(f, X), lax.rem(t, 2), t // 2
    partner = (f, t + 1 - 2 * c)
    rows = mean_q.shape[0]
    chunk = rows * X

    def zpeer(dz):
        return (lax.rem(z + dz, Z) * X + x, t)

    def xpeer(dx):
        return (z * X + lax.rem(x + dx, X), t)

    def ypeer(dy):
        return (f, lax.rem(y + dy, Y) * 2 + c)

    greet(
        [zpeer(d) for d in range(1, Z)]
        + [xpeer(d) for d in range(1, X)]
        + [ypeer(d) for d in range(1, Y)]
        + [partner]
    )
    sent = []

    def start(src, dst, send_sem, recv_sem, peer):
        copy = remote(src, dst, send_sem, recv_sem, peer)
        copy.start()
        sent.append(copy)

    def landed(dst, send_sem, recv_sem):
        remote(dst, dst, send_sem, recv_sem, partner).wait_recv()

    sides = (
        (parts_q, r1q, s1q, r2q, s2q, r3q, s3q, r4q),
        (parts_o, r1o, s1o, r2o, s2o, r3o, s3o, r4o),
    )
    gathers = (dq, do, wq_all, wo_all)
    heights = (rows, rows, wq.shape[0], wo.shape[0])

    def block(j, dz, dx):
        h = heights[j]
        b = lax.rem(z + Z - dz, Z) * X + lax.rem(x + X - dx, X)
        return gathers[j].at[pl.ds(pl.multiple_of(b * h, h), h), :]

    def spread(j, src):
        for dz in range(1, Z):
            start(src, block(j, 0, 0), gzs.at[j, dz], gzr.at[j, dz], zpeer(dz))
        for dx in range(1, X):
            start(src, block(j, 0, 0), gxs.at[j, 0, dx], gxr.at[j, 0, dx], xpeer(dx))

    def forward(j, dz):
        landed(block(j, dz, 0), gzs.at[j, dz], gzr.at[j, dz])
        for dx in range(1, X):
            start(block(j, dz, 0), block(j, dz, 0), gxs.at[j, dz, dx], gxr.at[j, dz, dx], xpeer(dx))

    def finish(j):
        for dz in range(Z):
            for dx in range(1, X):
                landed(block(j, dz, dx), gxs.at[j, dz, dx], gxr.at[j, dz, dx])

    order = [*range(1, Z), 0]

    def span(k):
        return pl.ds(pl.multiple_of(lax.rem(z + k, Z) * chunk, chunk), chunk)

    def columns(i, core, dy):
        width = sides[i][1].shape[-1]
        start_at = (lax.rem(y + dy, Y) * 2 + core) * width
        return pl.ds(pl.multiple_of(start_at, width), width)

    ys = [*range(1, Y), 0]
    for k in order:
        for dy in ys:
            for i in range(2):
                parts, r1 = sides[i][:2]
                start(
                    parts.at[span(k), columns(i, 1 - c, dy)], r1.at[dy, k],
                    s1s.at[i, dy, k], s1r.at[i, dy, k], partner,
                )
    for j, w in ((2, wq), (3, wo)):
        spread(j, w)
        h = heights[j]
        gathers[j][pl.ds(pl.multiple_of(f * h, h), h), :] = w[...]
    for k in order:
        for dy in ys:
            for i in range(2):
                parts, r1, s1, r2 = sides[i][:4]
                landed(r1.at[dy, k], s1s.at[i, dy, k], s1r.at[i, dy, k])
                s1[dy, k] = (parts[span(k), columns(i, c, dy)].astype(F32) + r1[dy, k].astype(F32)).astype(BF16)
                if dy:
                    start(s1.at[dy, k], r2.at[dy, k], s2s.at[i, dy, k], s2r.at[i, dy, k], ypeer(dy))

    def add_x(k):
        for i in range(2):
            s2, r3, s3, r4 = sides[i][4:]
            own = pl.ds(pl.multiple_of(x * rows, rows), rows)
            total = s2[k, own, :].astype(F32)
            for dx in range(1, X):
                landed(r3.at[dx, k], s3s.at[i, dx, k], s3r.at[i, dx, k])
                total += r3[dx, k].astype(F32)
            s3[k] = total.astype(BF16)
            if k:
                start(s3.at[k], r4.at[k], s4s.at[i, k], s4r.at[i, k], zpeer(k))

    for at, k in enumerate(order):
        for i in range(2):
            _, _, s1, r2, s2, r3 = sides[i][:6]
            total = s1[0, k].astype(F32)
            for dy in range(1, Y):
                landed(r2.at[dy, k], s2s.at[i, dy, k], s2r.at[i, dy, k])
                total += r2[dy, k].astype(F32)
            s2[k] = total.astype(BF16)
            for dx in range(1, X):
                there = pl.ds(pl.multiple_of(lax.rem(x + dx, X) * rows, rows), rows)
                start(s2.at[k, there, :], r3.at[dx, k], s3s.at[i, dx, k], s3r.at[i, dx, k], xpeer(dx))
        if at:
            add_x(order[at - 1])
    add_x(order[-1])
    for i, (mean, square, mean_new, square_new) in enumerate(
        ((mean_q, square_q, mq, sq), (mean_o, square_o, mo, so))
    ):
        s3, r4 = sides[i][6:]
        total = s3[0].astype(F32)
        for k in range(1, Z):
            landed(r4.at[k], s4s.at[i, k], s4r.at[i, k])
            total += r4[k].astype(F32)
        reduced = total * scale
        first = 0.8 * mean[...] + 0.2 * reduced
        second = 0.9 * square[...] + 0.1 * reduced * reduced
        mean_new[...] = first
        square_new[...] = second
        gathers[i][pl.ds(pl.multiple_of(f * rows, rows), rows), :] = (
            first / (jnp.sqrt(second) + 1e-08)
        ).astype(BF16)
        spread(i, block(i, 0, 0))
    for dz in range(1, Z):
        for j in (2, 3):
            forward(j, dz)
    for dz in range(1, Z):
        for j in (0, 1):
            forward(j, dz)
    for j in range(4):
        finish(j)
    for copy in sent:
        copy.wait_send()


def vmem(n):
    return [pl.BlockSpec(memory_space=pltpu.VMEM)] * n


def dma(*shape):
    return pltpu.SemaphoreType.DMA(shape)


def shards(
    normed_inputs, query_cotangent, head_outputs, output_cotangent, query_weight, out_weight,
    query_basis, out_basis, query_mean, query_square, out_mean, out_square,
):
    fs, tp = lax.axis_size("fs"), lax.axis_size("tp")
    Z, X = plane(fs)
    Y = tp // 2
    scale = (normed_inputs.shape[0] * fs * tp) ** (-0.5)
    model_rows, query_width = normed_inputs.shape[1], query_cotangent.shape[1]
    qc, oc = query_weight.shape[1], out_weight.shape[1]
    rows, rank = query_mean.shape[0], query_basis.shape[1]
    shape = jax.ShapeDtypeStruct
    query_all, out_all = pl.pallas_call(
        functools.partial(gather_basis, Z, X),
        out_shape=(shape((model_rows, rank), BF16), shape((query_width, rank), BF16)),
        in_specs=vmem(2),
        out_specs=vmem(2),
        scratch_shapes=[dma(2, Z), dma(2, Z), dma(2, Z, X), dma(2, Z, X), dma(2, Z, X), dma(2, Z, X)],
        compiler_params=pltpu.CompilerParams(collective_id=0, has_side_effects=True),
    )(query_basis, out_basis)
    contract = (((0,), (0,)), ((), ()))
    query_left = jnp.dot(normed_inputs, query_all, preferred_element_type=F32).astype(BF16)
    out_left = jnp.dot(head_outputs, out_all, preferred_element_type=F32).astype(BF16)
    parts_q = lax.dot_general(query_left, query_cotangent, contract, preferred_element_type=F32).astype(BF16)
    parts_o = lax.dot_general(out_left, output_cotangent, contract, preferred_element_type=F32).astype(BF16)

    def pair(*lead):
        return [pltpu.VMEM((*lead, qc), BF16), pltpu.VMEM((*lead, oc), BF16)]

    chunk = X * rows
    scratch = (
        pair(Y, Z, chunk) + pair(Y, Z, chunk) + pair(Y, Z, chunk) + pair(Z, chunk)
        + pair(X, Z, rows) + pair(Z, rows) + pair(Z, rows)
        + [dma(2, Y, Z)] * 4 + [dma(2, X, Z)] * 2 + [dma(2, Z)] * 2
        + [dma(4, Z)] * 2 + [dma(4, Z, X)] * 2
    )
    dq, do, mq, sq, mo, so, wq_all, wo_all = pl.pallas_call(
        functools.partial(update, Z, X, Y, scale),
        out_shape=(
            shape((rank, qc), BF16), shape((rank, oc), BF16),
            shape((rows, qc), F32), shape((rows, qc), F32),
            shape((rows, oc), F32), shape((rows, oc), F32),
            shape((model_rows, qc), BF16), shape((query_width, oc), BF16),
        ),
        in_specs=vmem(8),
        out_specs=vmem(8),
        scratch_shapes=scratch,
        compiler_params=pltpu.CompilerParams(collective_id=1, has_side_effects=True),
    )(
        parts_q, parts_o, query_weight.astype(BF16), out_weight.astype(BF16),
        query_mean, query_square, out_mean, out_square,
    )
    at = lax.axis_index("fs")

    def apply(basis, direction, weight, weight_all):
        full = jnp.dot(basis, direction, preferred_element_type=F32)
        gain = lax.rsqrt(jnp.sum(full * full, axis=0) / full.shape[0] + 0.05)
        copy = (weight_all.astype(F32) - 0.01 * (full * gain)).astype(BF16)
        step = lax.dynamic_slice_in_dim(full, at * weight.shape[0], weight.shape[0], 0) * gain
        return step, weight - 0.01 * step, copy

    query_out = apply(query_all, dq, query_weight, wq_all)
    out_out = apply(out_all, do, out_weight, wo_all)
    return (mq, sq, *query_out, mo, so, *out_out)


def solution(mesh):
    token = P(("fs", "tp"), None)
    both, row, column = P("fs", "tp"), P("fs", None), P(None, "tp")
    return jax.shard_map(
        shards,
        mesh=mesh,
        in_specs=(token,) * 4 + (both, both, row, row) + (both,) * 4,
        out_specs=(both, both, both, both, column) * 2,
        check_vma=False,
    )
```

time: 367 us -> 133 us (0.36)
  waiting for transfers between devices: 267 us -> 0 us
  Pallas kernels: 0 us -> 100 us
  blocking collectives: 51.6 us -> 0 us
  between operations: 14.2 us -> 0.75 us
    all_gather x5 -> x0, waiting for transfers between devices: 170 us -> none  [the longest x1 44.4 us: shards(): lax.all_gather(out_basis, 'fs', axis=0, tiled=True)]
    pallas_call x0 -> x2, Pallas kernels: none -> 100 us  [the longest x1 67.9 us: shards(): pl.pallas_call(functools.partial(update, Z, X, Y, scale), out_shape=(shap...]
    reduce_scatter x2 -> x0, waiting for transfers between devices: 95.3 us -> none  [the longest x1 73.1 us: shards(): lax.psum_scatter(jnp.concatenate([query_part.reshape(rank_rows * lax.axis...]
    all_gather x1 -> x0, blocking collectives: 32.6 us -> none  [shards(): query_piece = lax.all_gather(query_direction, 'fs', axis=0, tiled=True)]
    psum x1 -> x0, blocking collectives: 19.1 us -> none  [shards(): lax.psum((jnp.sum(query_full * query_full, axis=0), jnp.sum(out_full * ou...]
    sub x0 -> x2, other arithmetic: none -> 3.7 us  [apply(): return (step, weight - 0.01 * step, copy)]
    dot_general x8 -> x4, matrix products: 16.4 us -> 16.2 us  [the longest x1 7.15 us: shards(): lax.dot_general(query_left, query_cotangent, contract, preferred_element_...]
  transfers between devices with their start and end apart: 7 -> 0, of which waited for: 7 -> 0; matrix products, arithmetic and copies ran while one was open for 3% -> 0% of each run, Pallas kernels for 0% -> 0%
where the time goes in v1:
time: 133 us
  Pallas kernels  100 us (75%)
  matrix products  16.2 us (12%)
  other arithmetic  8.68 us (7%)
  local copies, waits for them, and re-layouts  7.02 us (5%)
    pallas_call x1, Pallas kernels, shards(): pl.pallas_call(functools.partial(update, Z, X, Y, scale), out_shape=(shap...  67.9 us
    pallas_call x1, Pallas kernels, shards(): pl.pallas_call(functools.partial(gather_basis, Z, X), out_shape=(shape((m...  32.1 us
    dot_general x1, matrix products, shards(): lax.dot_general(query_left, query_cotangent, contract, preferred_element_...  7.15 us
    unnamed x22, local copies, waits for them, and re-layouts  7.02 us
    dot_general x1, matrix products, shards(): lax.dot_general(out_left, output_cotangent, contract, preferred_element_t...  6.21 us
    sub x2, other arithmetic, apply(): return (step, weight - 0.01 * step, copy)  3.7 us
    dot_general x2, matrix products, apply(): full = jnp.dot(basis, direction, preferred_element_type=F32)  2.89 us
    convert_element_type x2, other arithmetic, apply(): copy = (weight_all.astype(F32) - 0.01 * (full * gain)).astype(BF16)  2.68 us

profile of v1, /device:TPU:0, one launch (start us, length us, event | category | flops | bytes accessed | tf_op | source)
XLA Modules:
  0.0 132.7 jit_solution(13042431762811496510)
XLA Ops:
  0.6 0.0 copy-start
  0.7 32.1 %shard_map.195 = (bf16[2048,512]{1,0:T(8,128)(2,1)}, bf16[1024,512]{1,0:T(8,128)(2,1)}) custom-call(bf16[256,512]{1,0:T(8,128)(2,1)} %qb.1, bf16[128,512]{1,0:T(8,128)(2,1)} %ob.1), custom_call_target="tpu_custom_call" | custom-call | tf_op jit(solution)/shard_map/pallas_call | solution.py:273
  32.8 6.2 %convolution_convert_fusion.parts_o = bf16[512,2048]{1,0:T(8,128)(2,1)} fusion(bf16[768,2048]{1,0:T(8,128)(2,1)S(1)} %copy-done, bf16[1024,512]{1,0:T(8,128)(2,1)} %get-tuple-element.21, bf16[768,1024]{1,0:T(8,128)(2,1)} %param.14), kind=kOutput, calls=%fused_computation | convolution fusion | flops 2417360896 | bytes 7864320 | tf_op jit(solution)/shard_map/dot_general | solution.py:285
  39.0 7.1 %convolution_convert_fusion.1.parts_q = bf16[512,1024]{1,0:T(8,128)(2,1)} fusion(bf16[768,1024]{1,0:T(8,128)(2,1)} %param.13, bf16[2048,512]{1,0:T(8,128)(2,1)} %get-tuple-element.20, bf16[768,2048]{1,0:T(8,128)(2,1)} %param.12), kind=kOutput, calls=%fused_computation.5 | convolution fusion | flops 2416836608 | bytes 7864320 | tf_op jit(solution)/shard_map/dot_general | solution.py:284
  46.1 0.7 convert_element_type.36.wq
  46.8 1.6 %convert_element_type.37.wo = bf16[128,512]{1,0:T(8,128)(2,1)} convert(f32[128,512]{1,0:T(8,128)} %param.17) | non-fusion elementwise | flops 65536 | bytes 393216 | tf_op jit(solution)/shard_map/convert_element_type | solution.py:310
  48.4 67.9 %shard_map.196 = (bf16[512,256]{1,0:T(8,128)(2,1)}, bf16[512,512]{1,0:T(8,128)(2,1)}, f32[64,256]{1,0:T(8,128)}, f32[64,256]{1,0:T(8,128)}, f32[64,512]{1,0:T(8,...) custom-call(bf16[512,1024]{1,0:T(8,128)(2,1)} %convolution_convert_fusion.1.parts_q, ...), custom_call_target="tpu_custom_call" | custom-call | tf_op jit(solution)/shard_map/pallas_call | solution.py:297
  116.4 2.2 %multiply_reduce_fusion = (f32[512]{0:T(512)S(1)}, f32[1024,512]{1,0:T(8,128)S(1)}) fusion(bf16[1024,512]{1,0:T(8,128)(2,1)} %get-tuple-element.21, bf16[512,512]{1,0:T(8,128)(2,1)} %get-tuple-element.28), kind=kOutput, calls=%fused_computation.2 | convolution fusion | flops 537918976 | bytes 3672064 | tf_op jit(solution)/shard_map/dot_general | solution.py:316
  118.6 0.0 copy-done.6
  118.6 0.0 copy-start.3
  118.6 0.0 copy-start.7
  118.6 1.4 %subtract_convert_fusion = bf16[1024,512]{1,0:T(8,128)(2,1)} fusion(f32[1024,512]{1,0:T(8,128)S(1)} %get-tuple-element.37, bf16[1024,512]{1,0:T(8,128)(2,1)S(1)} %copy-done.6, f32[512]{0:T(512)S(1)} %add_rsqrt_fusion), kind=kLoop, calls=%fused_computation.1 | loop fusion | flops 2621440 | bytes 4196352 | tf_op jit(solution)/shard_map/convert_element_type | solution.py:318
  120.0 0.3 copy-done.2
  120.2 1.1 copy-done.3
  121.3 0.7 multiply_reduce_fusion.1
  122.0 0.0 copy-start.1
  122.1 0.5 copy-done.4
  122.5 1.3 subtract_convert_fusion.1
  123.9 1.9 %multiply_subtract_fusion = (f32[128,512]{1,0:T(8,128)}, f32[128,512]{1,0:T(8,128)}) fusion(f32[128,512]{1,0:T(8,128)} %param.17, f32[512]{0:T(512)S(1)} %add_rsqrt_fusion, f32[1024,512]{1,0:T(8,128)} %copy-done.2, s32[]{:T(128)S(6)} %select_n.7), kind=kLoop, calls=%fused_computation.8 | loop fusion | flops 196608 | bytes 1050628 | tf_op jit(solution)/shard_map/sub | solution.py:320
  125.8 1.8 %multiply_subtract_fusion.1 = (f32[256,256]{1,0:T(8,128)}, f32[256,256]{1,0:T(8,128)}) fusion(f32[256,256]{1,0:T(8,128)S(1)} %copy-done.5, f32[256]{0:T(256)S(1)} %add_rsqrt_fusion.1, f32[2048,256]{1,0:T(8,128)} %copy-done.1, s32[]{:T(128)S(6)} %select_n.6), kind=kLoop, calls=%fused_computation.10 | loop fusion | flops 196608 | bytes 1049604 | tf_op jit(solution)/shard_map/sub | solution.py:320
  127.6 1.5 %copy.26 = f32[64,256]{1,0:T(8,128)} copy(f32[64,256]{1,0:T(8,128)} %get-tuple-element.48) | data formatting | bytes 131072
  129.0 1.5 %copy.27 = f32[64,256]{1,0:T(8,128)} copy(f32[64,256]{1,0:T(8,128)} %get-tuple-element.49) | data formatting | bytes 131072
  130.5 1.6 %copy.28 = f32[64,512]{1,0:T(8,128)} copy(f32[64,512]{1,0:T(8,128)} %get-tuple-element.53) | data formatting | bytes 262144
  132.1 0.7 copy.29
  (12 shorter events, 0.0 us)
Async XLA Ops:
  0.6 32.1 %copy-start = (bf16[768,2048]{1,0:T(8,128)(2,1)S(1)}, bf16[768,2048]{1,0:T(8,128)(2,1)}, u32[]{:S(2)}) copy-start(bf16[768,2048]{1,0:T(8,128)(2,1)} %param.15) | copy-start | bytes 9437188
  39.0 7.2 %copy-start.5 = (f32[256,256]{1,0:T(8,128)S(1)}, f32[256,256]{1,0:T(8,128)}, u32[]{:S(2)}) copy-start(f32[256,256]{1,0:T(8,128)} %param.16) | copy-start | bytes 786436
  116.4 2.2 %copy-start.6 = (bf16[1024,512]{1,0:T(8,128)(2,1)S(1)}, bf16[1024,512]{1,0:T(8,128)(2,1)}, u32[]{:S(2)}) copy-start(bf16[1024,512]{1,0:T(8,128)(2,1)} %get-tuple-element.29) | copy-start | bytes 3145732
  118.6 1.7 %copy-start.2 = (f32[1024,512]{1,0:T(8,128)}, f32[1024,512]{1,0:T(8,128)S(1)}, u32[]{:S(2)}) copy-start(f32[1024,512]{1,0:T(8,128)S(1)} %get-tuple-element.37) | copy-start | bytes 6291460
  118.6 2.7 %copy-start.3 = (bf16[2048,512]{1,0:T(8,128)(2,1)S(1)}, bf16[2048,512]{1,0:T(8,128)(2,1)}, u32[]{:S(2)}) copy-start(bf16[2048,512]{1,0:T(8,128)(2,1)} %get-tuple-element.20) | copy-start | bytes 6291460
  118.6 2.7 %copy-start.7 = (bf16[512,256]{1,0:T(8,128)(2,1)S(1)}, bf16[512,256]{1,0:T(8,128)(2,1)}, u32[]{:S(2)}) copy-start(bf16[512,256]{1,0:T(8,128)(2,1)} %get-tuple-element.24) | copy-start | bytes 786436
  121.3 1.2 copy-start.4
  122.0 1.8 %copy-start.1 = (f32[2048,256]{1,0:T(8,128)}, f32[2048,256]{1,0:T(8,128)S(1)}, u32[]{:S(2)}) copy-start(f32[2048,256]{1,0:T(8,128)S(1)} %get-tuple-element.35) | copy-start | bytes 6291460
  123.9 8.2 %copy-start.8 = (f32[64,512]{1,0:T(8,128)S(1)}, f32[64,512]{1,0:T(8,128)}, u32[]{:S(2)}) copy-start(f32[64,512]{1,0:T(8,128)} %get-tuple-element.54) | copy-start | bytes 393220

commit v2 on v1

--- a/solution.py
+++ b/solution.py
@@ -220,7 +220,12 @@
                 start(s2.at[k, there, :], r3.at[dx, k], s3s.at[i, dx, k], s3r.at[i, dx, k], xpeer(dx))
         if at:
             add_x(order[at - 1])
+        if at > 1:
+            for j in (2, 3):
+                forward(j, at - 1)
     add_x(order[-1])
+    for j in (2, 3):
+        forward(j, Z - 1)
     for i, (mean, square, mean_new, square_new) in enumerate(
         ((mean_q, square_q, mq, sq), (mean_o, square_o, mo, so))
     ):
@@ -238,9 +243,6 @@
             first / (jnp.sqrt(second) + 1e-08)
         ).astype(BF16)
         spread(i, block(i, 0, 0))
-    for dz in range(1, Z):
-        for j in (2, 3):
-            forward(j, dz)
     for dz in range(1, Z):
         for j in (0, 1):
             forward(j, dz)

time: 133 us -> 123 us (0.925)
  Pallas kernels: 100 us -> 90 us
    pallas_call x1, Pallas kernels: 67.9 us -> 57.9 us  [shards(): pl.pallas_call(functools.partial(update, Z, X, Y, scale), out_shape=(shap...]
where the time goes in v2:
time: 123 us
  Pallas kernels  90 us (73%)
  matrix products  16.2 us (13%)
  other arithmetic  8.68 us (7%)
  local copies, waits for them, and re-layouts  7.02 us (6%)
    pallas_call x1, Pallas kernels, shards(): pl.pallas_call(functools.partial(update, Z, X, Y, scale), out_shape=(shap...  57.9 us
    pallas_call x1, Pallas kernels, shards(): pl.pallas_call(functools.partial(gather_basis, Z, X), out_shape=(shape((m...  32.1 us
    dot_general x1, matrix products, shards(): lax.dot_general(query_left, query_cotangent, contract, preferred_element_...  7.15 us
    unnamed x22, local copies, waits for them, and re-layouts  7.02 us
    dot_general x1, matrix products, shards(): lax.dot_general(out_left, output_cotangent, contract, preferred_element_t...  6.21 us
    sub x2, other arithmetic, apply(): return (step, weight - 0.01 * step, copy)  3.7 us
    dot_general x2, matrix products, apply(): full = jnp.dot(basis, direction, preferred_element_type=F32)  2.88 us
    convert_element_type x2, other arithmetic, apply(): copy = (weight_all.astype(F32) - 0.01 * (full * gain)).astype(BF16)  2.68 us

profile of v2, /device:TPU:0, one launch (start us, length us, event | category | flops | bytes accessed | tf_op | source)
XLA Modules:
  0.0 122.7 jit_solution(16684155925383781662)
XLA Ops:
  0.6 0.0 copy-start
  0.7 32.1 %shard_map.195 = (bf16[2048,512]{1,0:T(8,128)(2,1)}, bf16[1024,512]{1,0:T(8,128)(2,1)}) custom-call(bf16[256,512]{1,0:T(8,128)(2,1)} %qb.1, bf16[128,512]{1,0:T(8,128)(2,1)} %ob.1), custom_call_target="tpu_custom_call" | custom-call | tf_op jit(solution)/shard_map/pallas_call | solution.py:275
  32.8 0.0 copy-done
  32.8 6.2 %convolution_convert_fusion.parts_o = bf16[512,2048]{1,0:T(8,128)(2,1)} fusion(bf16[768,2048]{1,0:T(8,128)(2,1)S(1)} %copy-done, bf16[1024,512]{1,0:T(8,128)(2,1)} %get-tuple-element.21, bf16[768,1024]{1,0:T(8,128)(2,1)} %param.14), kind=kOutput, calls=%fused_computation | convolution fusion | flops 2417360896 | bytes 7864320 | tf_op jit(solution)/shard_map/dot_general | solution.py:287
  39.0 7.1 %convolution_convert_fusion.1.parts_q = bf16[512,1024]{1,0:T(8,128)(2,1)} fusion(bf16[768,1024]{1,0:T(8,128)(2,1)} %param.13, bf16[2048,512]{1,0:T(8,128)(2,1)} %get-tuple-element.20, bf16[768,2048]{1,0:T(8,128)(2,1)} %param.12), kind=kOutput, calls=%fused_computation.5 | convolution fusion | flops 2416836608 | bytes 7864320 | tf_op jit(solution)/shard_map/dot_general | solution.py:286
  46.1 0.0 copy-done.5
  46.1 0.7 convert_element_type.36.wq
  46.8 1.6 %convert_element_type.37.wo = bf16[128,512]{1,0:T(8,128)(2,1)} convert(f32[128,512]{1,0:T(8,128)} %param.17) | non-fusion elementwise | flops 65536 | bytes 393216 | tf_op jit(solution)/shard_map/convert_element_type | solution.py:312
  48.4 57.9 %shard_map.196 = (bf16[512,256]{1,0:T(8,128)(2,1)}, bf16[512,512]{1,0:T(8,128)(2,1)}, f32[64,256]{1,0:T(8,128)}, f32[64,256]{1,0:T(8,128)}, f32[64,512]{1,0:T(8,...) custom-call(bf16[512,1024]{1,0:T(8,128)(2,1)} %convolution_convert_fusion.1.parts_q, ...), custom_call_target="tpu_custom_call" | custom-call | tf_op jit(solution)/shard_map/pallas_call | solution.py:299
  106.3 0.0 copy-start.6
  106.3 2.2 %multiply_reduce_fusion = (f32[512]{0:T(512)S(1)}, f32[1024,512]{1,0:T(8,128)S(1)}) fusion(bf16[1024,512]{1,0:T(8,128)(2,1)} %get-tuple-element.21, bf16[512,512]{1,0:T(8,128)(2,1)} %get-tuple-element.28), kind=kOutput, calls=%fused_computation.2 | convolution fusion | flops 537918976 | bytes 3672064 | tf_op jit(solution)/shard_map/dot_general | solution.py:318
  108.6 1.4 %subtract_convert_fusion = bf16[1024,512]{1,0:T(8,128)(2,1)} fusion(f32[1024,512]{1,0:T(8,128)S(1)} %get-tuple-element.37, bf16[1024,512]{1,0:T(8,128)(2,1)S(1)} %copy-done.6, f32[512]{0:T(512)S(1)} %add_rsqrt_fusion), kind=kLoop, calls=%fused_computation.1 | loop fusion | flops 2621440 | bytes 4196352 | tf_op jit(solution)/shard_map/convert_element_type | solution.py:320
  109.9 0.3 copy-done.2
  110.2 1.1 copy-done.3
  111.3 0.7 multiply_reduce_fusion.1
  112.0 0.0 copy-start.1
  112.0 0.5 copy-done.4
  112.5 1.3 %subtract_convert_fusion.1 = bf16[2048,256]{1,0:T(8,128)(2,1)} fusion(f32[2048,256]{1,0:T(8,128)S(1)} %get-tuple-element.35, bf16[2048,256]{1,0:T(8,128)(2,1)S(1)} %copy-done.4, f32[256]{0:T(256)S(1)} %add_rsqrt_fusion.1), kind=kLoop, calls=%fused_computation.3 | loop fusion | flops 2621440 | bytes 4195328 | tf_op jit(solution)/shard_map/convert_element_type | solution.py:320
  113.8 1.9 %multiply_subtract_fusion = (f32[128,512]{1,0:T(8,128)}, f32[128,512]{1,0:T(8,128)}) fusion(f32[128,512]{1,0:T(8,128)} %param.17, f32[512]{0:T(512)S(1)} %add_rsqrt_fusion, f32[1024,512]{1,0:T(8,128)} %copy-done.2, s32[]{:T(128)S(6)} %select_n.7), kind=kLoop, calls=%fused_computation.8 | loop fusion | flops 196608 | bytes 1050628 | tf_op jit(solution)/shard_map/sub | solution.py:322
  115.7 1.8 %multiply_subtract_fusion.1 = (f32[256,256]{1,0:T(8,128)}, f32[256,256]{1,0:T(8,128)}) fusion(f32[256,256]{1,0:T(8,128)S(1)} %copy-done.5, f32[256]{0:T(256)S(1)} %add_rsqrt_fusion.1, f32[2048,256]{1,0:T(8,128)} %copy-done.1, s32[]{:T(128)S(6)} %select_n.6), kind=kLoop, calls=%fused_computation.10 | loop fusion | flops 196608 | bytes 1049604 | tf_op jit(solution)/shard_map/sub | solution.py:322
  117.5 1.5 %copy.26 = f32[64,256]{1,0:T(8,128)} copy(f32[64,256]{1,0:T(8,128)} %get-tuple-element.48) | data formatting | bytes 131072
  119.0 1.5 %copy.27 = f32[64,256]{1,0:T(8,128)} copy(f32[64,256]{1,0:T(8,128)} %get-tuple-element.49) | data formatting | bytes 131072
  120.5 1.6 %copy.28 = f32[64,512]{1,0:T(8,128)} copy(f32[64,512]{1,0:T(8,128)} %get-tuple-element.53) | data formatting | bytes 262144
  122.0 0.7 copy.29
  (12 shorter events, 0.0 us)
Async XLA Ops:
  0.6 32.1 %copy-start = (bf16[768,2048]{1,0:T(8,128)(2,1)S(1)}, bf16[768,2048]{1,0:T(8,128)(2,1)}, u32[]{:S(2)}) copy-start(bf16[768,2048]{1,0:T(8,128)(2,1)} %param.15) | copy-start | bytes 9437188
  39.0 7.2 %copy-start.5 = (f32[256,256]{1,0:T(8,128)S(1)}, f32[256,256]{1,0:T(8,128)}, u32[]{:S(2)}) copy-start(f32[256,256]{1,0:T(8,128)} %param.16) | copy-start | bytes 786436
  106.3 2.2 %copy-start.6 = (bf16[1024,512]{1,0:T(8,128)(2,1)S(1)}, bf16[1024,512]{1,0:T(8,128)(2,1)}, u32[]{:S(2)}) copy-start(bf16[1024,512]{1,0:T(8,128)(2,1)} %get-tuple-element.29) | copy-start | bytes 3145732
  108.5 1.7 %copy-start.2 = (f32[1024,512]{1,0:T(8,128)}, f32[1024,512]{1,0:T(8,128)S(1)}, u32[]{:S(2)}) copy-start(f32[1024,512]{1,0:T(8,128)S(1)} %get-tuple-element.37) | copy-start | bytes 6291460
  108.5 2.7 %copy-start.3 = (bf16[2048,512]{1,0:T(8,128)(2,1)S(1)}, bf16[2048,512]{1,0:T(8,128)(2,1)}, u32[]{:S(2)}) copy-start(bf16[2048,512]{1,0:T(8,128)(2,1)} %get-tuple-element.20) | copy-start | bytes 6291460
  108.6 2.7 %copy-start.7 = (bf16[512,256]{1,0:T(8,128)(2,1)S(1)}, bf16[512,256]{1,0:T(8,128)(2,1)}, u32[]{:S(2)}) copy-start(bf16[512,256]{1,0:T(8,128)(2,1)} %get-tuple-element.24) | copy-start | bytes 786436
  111.3 1.2 copy-start.4
  112.0 1.8 %copy-start.1 = (f32[2048,256]{1,0:T(8,128)}, f32[2048,256]{1,0:T(8,128)S(1)}, u32[]{:S(2)}) copy-start(f32[2048,256]{1,0:T(8,128)S(1)} %get-tuple-element.35) | copy-start | bytes 6291460
  113.8 8.2 %copy-start.8 = (f32[64,512]{1,0:T(8,128)S(1)}, f32[64,512]{1,0:T(8,128)}, u32[]{:S(2)}) copy-start(f32[64,512]{1,0:T(8,128)} %get-tuple-element.54) | copy-start | bytes 393220
